TPU v7x, 256 devices: a whole 4x4x8 slice. The times are simulated.
256 devices in a mesh: sp: 16 (over y, x), dp: 16 (over z, core).
Axes of the slice: x: 4, y: 4, z: 8, core: 2. Of those that a mesh axis runs over, the one named last changes fastest.
Arguments:
- tokens: bfloat16 [16, 6144, 2048], P('dp', 'sp'), may hold values from -6 to 6
- value_act: bfloat16 [16, 6144, 1024], P('dp', 'sp'), may hold values from -6 to 6
- gate_act: bfloat16 [16, 6144, 1024], P('dp', 'sp'), may hold values from -6 to 6
- cotangent: bfloat16 [16, 6144, 1024], P('dp', 'sp'), may hold values from -6 to 6
- value_weight: bfloat16 [2048, 1024], P('dp'), may hold values from -0.1875 to 0.1875
- gate_weight: bfloat16 [2048, 1024], P('dp'), may hold values from -0.1875 to 0.1875
- norm_gain: float32 [1024], replicated, may hold values from 0.1 to 1.9
- norm_bias: float32 [1024], replicated, may hold values from -3 to 3
- mix_weight: bfloat16 [16, 128, 128], replicated, may hold values from -0.5 to 0.5
- mix_bias: float32 [16, 128], replicated, may hold values from 0.1 to 1.9
Outputs:
- tokens_grad: bfloat16 [16, 6144, 2048], P('dp', 'sp')
- value_weight_grad: float32 [2048, 1024], P('dp')
- gate_weight_grad: float32 [2048, 1024], P('dp')
- mix_weight_grad: float32 [16, 128, 128], replicated
- mix_bias_grad: float32 [16, 128], replicated
- norm_gain_grad: float32 [1024], replicated
- norm_bias_grad: float32 [1024], replicated
All inputs are finite; a program needn't handle non-finite values.
Results may differ from a plain program's by a relative error of at most 0.0054.
Values may be sent and summed in bfloat16 or wider, within the bound.
A program may use at most 128 MiB of HBM per device.

v0:
```python
import jax
import jax.numpy as jnp
from jax import lax
from jax.sharding import PartitionSpec as P

EPSILON = 1e-06


def gelu_slope(values):
    cdf_part = 0.5 * (1.0 + lax.erf(values * 0.7071067811865476))
    pdf_part = jnp.exp(-0.5 * values * values) * 0.3989422804014327
    return cdf_part + values * pdf_part


def mixer_backward(value_act, gate_act, cotangent, norm_gain, norm_bias, mix_weight, mix_bias):
    seq_len, channels = value_act.shape
    groups, block_len = (mix_weight.shape[0], mix_weight.shape[1])
    group_dim = channels // groups
    blocks = seq_len // block_len
    value_float = value_act.astype(jnp.float32)
    gate_float = gate_act.astype(jnp.float32)
    activated = jax.nn.gelu(value_float, approximate=False)
    gate_gelu = jax.nn.gelu(gate_float, approximate=False)
    centred = gate_gelu - jnp.mean(gate_gelu, axis=-1, keepdims=True)
    inv_std = lax.rsqrt(jnp.mean(centred * centred, axis=-1, keepdims=True) + EPSILON)
    normed = centred * inv_std
    spread_in = (normed * norm_gain + norm_bias).astype(jnp.bfloat16)
    spread_in = spread_in.reshape(blocks, block_len, groups, group_dim)
    causal = jnp.tril(jnp.ones((block_len, block_len), dtype=bool))
    masked_weight = jnp.where(causal[None], mix_weight, jnp.zeros_like(mix_weight))
    spatial = jnp.einsum(
        "gts,bsgd->btgd", masked_weight, spread_in, preferred_element_type=jnp.float32
    )
    spatial = (spatial + mix_bias.T[None, :, :, None]).reshape(seq_len, channels)
    grad_out = cotangent.astype(jnp.float32)
    grad_act = grad_out * spatial
    grad_spatial = grad_out * activated
    grad_split = grad_spatial.reshape(blocks, block_len, groups, group_dim)
    bias_grad = jnp.sum(grad_split, axis=(0, 3)).T
    spatial_low = grad_split.astype(jnp.bfloat16)
    weight_grad = jnp.einsum(
        "btgd,bsgd->gts", spatial_low, spread_in, preferred_element_type=jnp.float32
    )
    weight_grad = jnp.where(causal[None], weight_grad, jnp.zeros_like(weight_grad))
    grad_norm = jnp.einsum(
        "gts,btgd->bsgd", masked_weight, spatial_low, preferred_element_type=jnp.float32
    )
    grad_norm = grad_norm.reshape(seq_len, channels)
    gain_grad = jnp.sum(grad_norm * normed, axis=0)
    shift_grad = jnp.sum(grad_norm, axis=0)
    grad_hat = grad_norm * norm_gain
    grad_gate = inv_std * (
        grad_hat
        - jnp.mean(grad_hat, axis=-1, keepdims=True)
        - normed * jnp.mean(grad_hat * normed, axis=-1, keepdims=True)
    )
    value_grad = (grad_act * gelu_slope(value_float)).astype(jnp.bfloat16)
    gate_grad = (grad_gate * gelu_slope(gate_float)).astype(jnp.bfloat16)
    return (value_grad, gate_grad, (weight_grad, bias_grad, gain_grad, shift_grad))


def shards(
    tokens,
    value_act,
    gate_act,
    cotangent,
    value_weight,
    gate_weight,
    norm_gain,
    norm_bias,
    mix_weight,
    mix_bias,
):
    value_grad, gate_grad, stats = mixer_backward(
        value_act[0], gate_act[0], cotangent[0], norm_gain, norm_bias, mix_weight, mix_bias
    )
    channels = value_grad.shape[1]
    both_grads = jnp.concatenate((value_grad, gate_grad), axis=1)
    both_weights = jnp.concatenate((value_weight, gate_weight), axis=1)
    input_grad = lax.dot_general(
        both_grads,
        lax.all_gather(both_weights, "dp", axis=0, tiled=True),
        (((1,), (1,)), ((), ())),
        preferred_element_type=jnp.float32,
    ).astype(jnp.bfloat16)
    inputs = tokens[0]
    shard_terms = lax.psum_scatter(
        lax.dot_general(
            inputs, both_grads, (((0,), (0,)), ((), ())), preferred_element_type=jnp.float32
        ),
        "dp",
        scatter_dimension=0,
        tiled=True,
    )
    weight_sums = lax.psum(shard_terms, "sp")
    totals = lax.psum((stats[0], stats[1], stats[2], stats[3]), ("sp", "dp"))
    return (
        input_grad[None],
        weight_sums[:, :channels],
        weight_sums[:, channels:],
        totals[0],
        totals[1],
        totals[2],
        totals[3],
    )


def solution(mesh):
    placed = (
        P("dp", "sp", None),
        P("dp", "sp", None),
        P("dp", "sp", None),
        P("dp", "sp", None),
        P("dp", None),
        P("dp", None),
        P(),
        P(),
        P(),
        P(),
    )
    return jax.shard_map(
        shards,
        mesh=mesh,
        in_specs=placed,
        out_specs=(P("dp", "sp", None), P("dp", None), P("dp", None), P(), P(), P(), P()),
        check_vma=False,
    )
```

profile of v0, /device:TPU:2, one launch (start us, length us, event | category | flops | bytes accessed | tf_op | source)
XLA Modules:
  0.0 603.1 jit_solution(7592910926025882119)
XLA Ops:
  7.2 2.4 copy.20
  9.6 4.5 fusion.96
  14.2 1.9 convert_multiply_fusion.1
  16.2 2.3 copy.28
  18.5 2.3 copy.19
  21.1 3.4 reshape.153
  24.6 3.0 convert_multiply_fusion
  27.6 3.6 mul.200
  31.1 3.6 mul.202
  34.7 3.6 mul.177
  38.3 3.6 mul.179
  41.9 5.6 fusion.93
  47.6 4.0 multiply_reduce_fusion
  51.7 1.1 copy-done.5
  53.4 1.1 copy.27
  54.7 0.8 fusion.78
  55.5 1.1 copy.36
  56.9 1.5 fusion.79
  58.5 0.9 copy-done.8
  59.4 9.4 %convolution_bitcast_fusion = f32[2048,2048]{0,1:T(8,128)} fusion(bf16[1,384,2048]{2,1,0:T(8,128)(2,1)S(1)} %copy-done, bf16[384,1024]{0,1:T(8,128)(2,1)S(1)} %fusion.79, bf16[384,1024]{0,1:T(8,128)(2,1)S(1)} %fusion.78), kind=kOutput, calls=%fused_computation | convolution fusion | flops 3224371200 | bytes 19922944 | tf_op jit(solution)/shard_map/dot_general | solution.py:88
  68.8 0.9 copy-done.13
  69.7 1.8 pad_maximum_fusion.3
  71.5 100.9 %reduce-scatter.2.cloned.1.call-done = f32[128,2048]{0,1:T(8,128)} async-done(((f32[2048,2048]{0,1:T(8,128)}), f32[128,2048]{0,1:T(8,128)}) %reduce-scatter.2.cloned.1.call-update) | async-done | bytes 1048592 | tf_op jit(solution)/shard_map/reduce_scatter | solution.py:87
  172.7 2.9 fusion.80
  175.8 77.8 %all-reduce = (f32[16,128]{1,0:T(8,128)}, f32[1024]{0:T(1024)}, f32[1024]{0:T(1024)}) all-reduce(f32[16,128]{1,0:T(8,128)S(1)} %bitcast.235, f32[1024]{0:T(1024)S(1)} %reduce_sum.73, f32[1024]{0:T(1024)S(1)} %reduce_sum.75), channel_id=1, replica_groups=mesh['sp'=16,'dp'=16] {'sp','dp'}, use_global_device_ids=true, to_apply=%region_8.9 | all-reduce | flops 4096 | bytes 32768 | tf_op jit(solution)/shard_map/psum | solution.py:96
  253.6 8.6 %fusion = bf16[1,384,2048]{2,1,0:T(8,128)(2,1)} fusion(bf16[2048,2048]{1,0:T(8,128)(2,1)} %all-gather.2.cloned.1.call-done, bf16[384,1024]{0,1:T(8,128)(2,1)} %copy-done.8, bf16[384,1024]{0,1:T(8,128)(2,1)} %copy-done.7), kind=kOutput, calls=%fused_computation.2 | convolution fusion | flops 3225157632 | bytes 11534336 | tf_op jit(solution)/shard_map/dot_general | solution.py:80
  262.2 67.5 %all-reduce.4.cloned.1.call-done = f32[128,2048]{0,1:T(8,128)} async-done(((f32[128,2048]{0,1:T(8,128)}), f32[128,2048]{0,1:T(8,128)}) %all-reduce.4.cloned.1.call-update) | async-done | bytes 1048592 | tf_op jit(solution)/shard_map/psum | solution.py:95
  329.6 1.3 fusion.98
  330.9 1.0 copy.38
  331.9 1.0 copy.37
  332.9 261.4 %all-reduce.6.cloned.1.call-done = f32[16,128,128]{2,1,0:T(8,128)} async-done(((f32[16,128,128]{2,1,0:T(8,128)}), f32[16,128,128]{2,1,0:T(8,128)}) %all-reduce.6.cloned.1.call-update) | async-done | bytes 1048592 | tf_op jit(solution)/shard_map/psum | solution.py:96
  594.3 2.3 copy.61
  (50 shorter events, 2.1 us)
Async XLA Ops:
  7.2 52.2 %copy-start = (bf16[1,384,2048]{2,1,0:T(8,128)(2,1)S(1)}, bf16[1,384,2048]{2,1,0:T(8,128)(2,1)}, u32[]{:S(2)}) copy-start(bf16[1,384,2048]{2,1,0:T(8,128)(2,1)} %param.10) | copy-start | bytes 4718596
  7.2 165.2 %reduce-scatter.2.cloned.1.call-start = ((), (), s32[]{:S(2)}) async-start(), calls=%async_computation.2 | async-start | bytes 17825792 | tf_op jit(solution)/shard_map/reduce_scatter | solution.py:87
  9.6 4.5 copy-start.1
  14.2 1.9 copy-start.14
  14.2 2.0 copy-start.16
  41.9 5.6 copy-start.10
  41.9 5.6 copy-start.11
  41.9 5.7 copy-start.12
  47.6 4.1 copy-start.9
  47.6 5.2 copy-start.15
  51.6 1.1 copy-start.5
  53.3 1.1 copy-start.3
  53.3 1.4 copy-start.4
  55.5 2.9 copy-start.7
  55.5 1.4 copy-start.2
  58.4 0.9 copy-start.8
  68.7 0.9 copy-start.13
  68.8 103.9 %copy-start.6 = (f32[3,128,16,64]{1,3,0,2:T(8,128)S(1)}, f32[3,128,16,64]{1,3,0,2:T(8,128)}, u32[]{:S(2)}) copy-start(f32[3,128,16,64]{1,3,0,2:T(8,128)} %copy-done.5) | copy-start | bytes 4718596
  68.8 184.8 %all-gather.2.cloned.1.call-start = ((), (), s32[]{:S(2)}) async-start(), calls=%async_computation.1 | async-start | bytes 8912896 | tf_op jit(solution)/shard_map/all_gather | solution.py:82
  71.5 258.2 %all-reduce.4.cloned.1.call-start = ((), (), s32[]{:S(2)}) async-start(), calls=%async_computation.3 | async-start | bytes 2097152 | tf_op jit(solution)/shard_map/psum | solution.py:95
  172.4 421.8 %all-reduce.6.cloned.1.call-start = ((), (), s32[]{:S(2)}) async-start(), calls=%async_computation.4 | async-start | bytes 2097152 | tf_op jit(solution)/shard_map/psum | solution.py:96
Sparse Core Ops, SparseCore 0:
  68.9 103.4 reduce-scatter.1
  174.8 55.9 all-gather.1
  234.0 95.5 all-reduce.3
  335.5 258.7 all-reduce.5
where the time goes:
time: 604 us; the launch traced here: 603 us
  waiting for transfers between devices  430 us (71%)
  blocking collectives  77.8 us (13%)
  local copies, waits for them, and re-layouts  36.4 us (6%)
  matrix products  25.4 us (4%)
  other arithmetic  19.3 us (3%)
  between operations  14 us (2%)
    psum x1, waiting for transfers between devices, shards(): totals = lax.psum((stats[0], stats[1], stats[2], stats[3]), ('sp', 'dp'))  261 us
    reduce_scatter x1, waiting for transfers between devices, shards(): lax.psum_scatter(lax.dot_general(inputs, both_grads, (((0,), (0,)), ((),...  101 us
    psum x1, blocking collectives, shards(): totals = lax.psum((stats[0], stats[1], stats[2], stats[3]), ('sp', 'dp'))  77.8 us
    psum x1, waiting for transfers between devices, shards(): weight_sums = lax.psum(shard_terms, 'sp')  67.5 us
    unnamed x40, local copies, waits for them, and re-layouts  14.9 us
  transfers between devices with their start and end apart: 4, of which 3 were waited for; matrix products, arithmetic and copies ran while one was open for 3% of the time, Pallas kernels for 0%

commit v1 on v0

--- a/solution.py
+++ b/solution.py
@@ -93,7 +93,9 @@
         tiled=True,
     )
     weight_sums = lax.psum(shard_terms, "sp")
-    totals = lax.psum((stats[0], stats[1], stats[2], stats[3]), ("sp", "dp"))
+    totals = (stats[0], stats[1], stats[2], stats[3])
+    for dd in ("sp", "dp"):
+        totals = lax.psum(totals, dd)
     return (
         input_grad[None],
         weight_sums[:, :channels],

time: 604 us -> 458 us (0.76)
  waiting for transfers between devices: 430 us -> 248 us
  blocking collectives: 77.8 us -> 116 us
    psum x1, waiting for transfers between devices: 261 us -> 103 us  [shards(): totals = lax.psum(totals, dd)]
    psum x1, waiting for transfers between devices: 67.5 us -> 0.01 us  [shards(): weight_sums = lax.psum(shard_terms, 'sp')]
    all_gather x1, waiting for transfers between devices: 0.01 us -> 45 us  [shards(): lax.all_gather(both_weights, 'dp', axis=0, tiled=True)]
    psum x1 -> x2, blocking collectives: 77.8 us -> 116 us  [shards(): totals = lax.psum(totals, dd)]
    unnamed x40 -> x52, local copies, waits for them, and re-layouts: 14.9 us -> 15.6 us
where the time goes in v1:
time: 458 us; the launch traced here: 456 us
  waiting for transfers between devices  248 us (54%)
  blocking collectives  116 us (25%)
  local copies, waits for them, and re-layouts  36 us (8%)
  matrix products  23.7 us (5%)
  other arithmetic  18.4 us (4%)
  between operations  14 us (3%)
    psum x2, blocking collectives, shards(): totals = lax.psum(totals, dd)  116 us
    psum x1, waiting for transfers between devices, shards(): totals = lax.psum(totals, dd)  103 us
    reduce_scatter x1, waiting for transfers between devices, shards(): lax.psum_scatter(lax.dot_general(inputs, both_grads, (((0,), (0,)), ((),...  100 us
    all_gather x1, waiting for transfers between devices, shards(): lax.all_gather(both_weights, 'dp', axis=0, tiled=True)  45 us
    unnamed x52, local copies, waits for them, and re-layouts  15.6 us
    dot_general x1, matrix products, shards(): lax.dot_general(inputs, both_grads, (((0,), (0,)), ((), ())), preferred_e...  9.37 us
  transfers between devices with their start and end apart: 4, of which 3 were waited for; matrix products, arithmetic and copies ran while one was open for 3% of the time, Pallas kernels for 0%

profile of v1, /device:TPU:2, one launch (start us, length us, event | category | flops | bytes accessed | tf_op | source)
XLA Modules:
  0.0 456.4 jit_solution(14912585025921948953)
XLA Ops:
  7.3 2.4 copy.20
  9.6 4.5 fusion.96
  14.2 1.9 convert_multiply_fusion.1
  16.2 2.3 copy.28
  18.5 2.4 copy.19
  21.2 3.5 reshape.153
  24.6 3.0 convert_multiply_fusion
  27.6 3.6 mul.200
  31.2 3.6 mul.202
  34.8 3.6 mul.177
  38.4 3.6 mul.179
  42.0 5.6 %fusion.93 = (f32[128,16]{0,1:T(8,128)S(1)}, bf16[3,128,16,64]{1,3,0,2:T(8,128)(2,1)S(1)}) fusion(f32[3,128,16,64]{1,0,3,2:T(4,128)} %mul.202, f32[3,128,16,64]{1,0,3,2:T(4,128)} %mul.200, f32[3,128,16,64]{1,0,3,2:T(4,128)} %reshape.153), kind=kLoop, calls=%fused_computation.137 | loop fusion | flops 25163776 | bytes 5513216 | tf_op jit(solution)/shard_map/reduce_sum | solution.py:39
  47.7 4.0 multiply_reduce_fusion
  51.7 1.1 copy-done.6
  53.4 1.1 copy.27
  54.8 0.8 fusion.78
  55.6 1.1 copy.36
  57.0 1.5 fusion.79
  58.5 0.9 copy-done.10
  59.4 9.4 %convolution_bitcast_fusion = f32[2048,2048]{0,1:T(8,128)} fusion(bf16[1,384,2048]{2,1,0:T(8,128)(2,1)S(1)} %copy-done, bf16[384,1024]{0,1:T(8,128)(2,1)S(1)} %fusion.79, bf16[384,1024]{0,1:T(8,128)(2,1)S(1)} %fusion.78), kind=kOutput, calls=%fused_computation | convolution fusion | flops 3224371200 | bytes 19922944 | tf_op jit(solution)/shard_map/dot_general | solution.py:88
  68.9 1.3 copy-done.7
  70.4 1.8 fusion.80
  72.2 100.3 %reduce-scatter.2.cloned.1.call-done = f32[128,2048]{0,1:T(8,128)} async-done(((f32[2048,2048]{0,1:T(8,128)}), f32[128,2048]{0,1:T(8,128)}) %reduce-scatter.2.cloned.1.call-update) | async-done | bytes 1048592 | tf_op jit(solution)/shard_map/reduce_scatter | solution.py:87
  172.8 0.8 pad_maximum_fusion.3
  173.9 69.5 %all-reduce.1 = (f32[16,128]{1,0:T(8,128)S(1)}, f32[1024]{0:T(1024)S(1)}, f32[1024]{0:T(1024)S(1)}) all-reduce(f32[16,128]{1,0:T(8,128)S(1)} %bitcast.235, f32[1024]{0:T(1024)S(1)} %reduce_sum.73, f32[1024]{0:T(1024)S(1)} %reduce_sum.75), channel_id=1, replica_groups=mesh['sp'=16,'dp'=16] {'sp'}, use_global_device_ids=true, to_apply=%region_9.10 | all-reduce | flops 4096 | bytes 32768 | tf_op jit(solution)/shard_map/psum | solution.py:98
  243.3 46.2 %all-reduce = (f32[16,128]{1,0:T(8,128)}, f32[1024]{0:T(1024)}, f32[1024]{0:T(1024)}) all-reduce(f32[16,128]{1,0:T(8,128)S(1)} %get-tuple-element.28, f32[1024]{0:T(1024)S(1)} %get-tuple-element.29, f32[1024]{0:T(1024)S(1)} %get-tuple-element.30), channel_id=1, replica_groups=mesh['sp'=16,'dp'=16] {'dp'}, use_global_device_ids=true, to_apply=%region_10.11 | all-reduce | flops 4096 | bytes 32768 | tf_op jit(solution)/shard_map/psum | solution.py:98
  289.6 45.0 %all-gather.2.cloned.1.call-done = bf16[2048,2048]{1,0:T(8,128)(2,1)} async-done(((bf16[128,2048]{1,0:T(8,128)(2,1)}), bf16[2048,2048]{1,0:T(8,128)(2,1)}) %all-gather.2.cloned.1.call-update) | async-done | bytes 8388624 | tf_op jit(solution)/shard_map/all_gather | solution.py:82
  334.5 8.0 %fusion = bf16[1,384,2048]{2,1,0:T(8,128)(2,1)} fusion(bf16[2048,2048]{1,0:T(8,128)(2,1)} %all-gather.2.cloned.1.call-done, bf16[384,1024]{0,1:T(8,128)(2,1)S(1)} %copy-done.11, bf16[384,1024]{0,1:T(8,128)(2,1)S(1)} %copy-done.9), kind=kOutput, calls=%fused_computation.2 | convolution fusion | flops 3225157632 | bytes 11534336 | tf_op jit(solution)/shard_map/dot_general | solution.py:80
  342.6 1.0 copy.38
  343.6 1.0 copy.37
  344.6 102.9 %all-reduce.6.cloned.1.call-done = f32[16,128,128]{2,1,0:T(8,128)} async-done(((f32[16,128,128]{2,1,0:T(8,128)}), f32[16,128,128]{2,1,0:T(8,128)}) %all-reduce.6.cloned.1.call-update) | async-done | bytes 1048592 | tf_op jit(solution)/shard_map/psum | solution.py:98
  447.5 2.3 copy.62
  (63 shorter events, 2.4 us)
Async XLA Ops:
  7.2 52.3 %copy-start = (bf16[1,384,2048]{2,1,0:T(8,128)(2,1)S(1)}, bf16[1,384,2048]{2,1,0:T(8,128)(2,1)}, u32[]{:S(2)}) copy-start(bf16[1,384,2048]{2,1,0:T(8,128)(2,1)} %param.10) | copy-start | bytes 4718596
  7.2 165.3 %reduce-scatter.2.cloned.1.call-start = ((), (), s32[]{:S(2)}) async-start(), calls=%async_computation.2 | async-start | bytes 17825792 | tf_op jit(solution)/shard_map/reduce_scatter | solution.py:87
  9.6 4.5 copy-start.2
  14.2 1.9 copy-start.20
  14.2 2.0 copy-start.22
  42.0 5.6 %copy-start.14 = (f32[3,128,16,64]{1,0,3,2:T(4,128)S(1)}, f32[3,128,16,64]{1,0,3,2:T(4,128)}, u32[]{:S(2)}) copy-start(f32[3,128,16,64]{1,0,3,2:T(4,128)} %mul.177) | copy-start | bytes 4718596
  42.0 5.6 %copy-start.15 = (f32[3,128,16,64]{1,0,3,2:T(4,128)S(1)}, f32[3,128,16,64]{1,0,3,2:T(4,128)}, u32[]{:S(2)}) copy-start(f32[3,128,16,64]{1,0,3,2:T(4,128)} %mul.179) | copy-start | bytes 4718596
  42.0 5.7 %copy-start.17 = (bf16[16,128,128]{2,1,0:T(8,128)(2,1)S(1)}, bf16[16,128,128]{2,1,0:T(8,128)(2,1)}, u32[]{:S(2)}) copy-start(bf16[16,128,128]{2,1,0:T(8,128)(2,1)} %param.18) | copy-start | bytes 1572868
  47.6 4.1 copy-start.12
  47.7 5.2 %copy-start.21 = (f32[16,128]{1,0:T(8,128)S(1)}, f32[16,128]{1,0:T(8,128)}, u32[]{:S(2)}) copy-start(f32[16,128]{1,0:T(8,128)} %param.19) | copy-start | bytes 24580
  51.7 1.1 copy-start.6
  53.4 1.1 copy-start.4
  53.4 1.4 copy-start.5
  55.6 2.9 copy-start.8
  55.6 1.4 copy-start.3
  58.5 0.9 copy-start.10
  68.8 1.4 copy-start.7
  68.8 1.6 copy-start.13
  68.8 220.7 %all-reduce.8.cloned.1.call-start = ((), (), s32[]{:S(2)}) async-start(), calls=%async_computation.4 | async-start | bytes 4194304 | tf_op jit(solution)/shard_map/psum | solution.py:95
  72.2 100.6 %copy-start.18 = (bf16[128,1024]{1,0:T(8,128)(2,1)S(1)}, bf16[128,1024]{1,0:T(8,128)(2,1)}, u32[]{:S(2)}) copy-start(bf16[128,1024]{1,0:T(8,128)(2,1)} %param.15) | copy-start | bytes 786436
  72.2 100.6 %copy-start.19 = (bf16[128,1024]{1,0:T(8,128)(2,1)S(1)}, bf16[128,1024]{1,0:T(8,128)(2,1)}, u32[]{:S(2)}) copy-start(bf16[128,1024]{1,0:T(8,128)(2,1)} %param.14) | copy-start | bytes 786436
  172.5 162.0 %copy-start.9 = (bf16[384,1024]{0,1:T(8,128)(2,1)S(1)}, bf16[384,1024]{0,1:T(8,128)(2,1)}, u32[]{:S(2)}) copy-start(bf16[384,1024]{0,1:T(8,128)(2,1)} %copy-done.8) | copy-start | bytes 2359300
  172.5 162.0 %copy-start.11 = (bf16[384,1024]{0,1:T(8,128)(2,1)S(1)}, bf16[384,1024]{0,1:T(8,128)(2,1)}, u32[]{:S(2)}) copy-start(bf16[384,1024]{0,1:T(8,128)(2,1)} %copy-done.10) | copy-start | bytes 2359300
  172.5 162.0 %all-gather.2.cloned.1.call-start = ((), (), s32[]{:S(2)}) async-start(), calls=%async_computation.1 | async-start | bytes 8912896 | tf_op jit(solution)/shard_map/all_gather | solution.py:82
  173.7 273.9 %all-reduce.6.cloned.1.call-start = ((), (), s32[]{:S(2)}) async-start(), calls=%async_computation.3 | async-start | bytes 2097152 | tf_op jit(solution)/shard_map/psum | solution.py:98
  289.6 53.0 %copy-start.16 = (f32[128,2048]{0,1:T(8,128)S(1)}, f32[128,2048]{0,1:T(8,128)}, u32[]{:S(2)}) copy-start(f32[128,2048]{0,1:T(8,128)} %get-tuple-element.31) | copy-start | bytes 3145732
  343.6 106.2 %copy-start.1 = (bf16[1,384,2048]{2,1,0:T(8,128)(2,1)S(1)}, bf16[1,384,2048]{2,1,0:T(8,128)(2,1)}, u32[]{:S(2)}) copy-start(bf16[1,384,2048]{2,1,0:T(8,128)(2,1)} %param.10) | copy-start | bytes 4718596
Sparse Core Ops, SparseCore 0:
  68.9 103.4 reduce-scatter.1
  176.4 99.9 all-reduce.7
  278.8 55.6 all-gather.1
  336.7 110.7 all-reduce.5
